TPU v7x, 32 devices: a whole 2x2x4 slice. The times are simulated.
32 devices in a mesh: fs: 16 (over z, y, x), tp: 2 (over core).
Axes of the slice: x: 2, y: 2, z: 4, core: 2. Of those that a mesh axis runs over, the one named last changes fastest.
Arguments:
- fwd_input: bfloat16 [2048, 2048], P('fs'), may hold values from -6 to 6
- saved_input: bfloat16 [2048, 2048], P('fs'), may hold values from -6 to 6
- out_cotangent: bfloat16 [2048, 2048], P('fs'), may hold values from -6 to 6
- up_weight: bfloat16 [2048, 4096], P('fs', 'tp'), may hold values from -0.125 to 0.125
- down_weight: bfloat16 [4096, 2048], P('tp', 'fs'), may hold values from -0.09375 to 0.09375
- up_grad_sum: float32 [2048, 4096], P('fs', 'tp'), may hold values from -6 to 6
Outputs:
- layer_out: bfloat16 [2048, 2048], P('fs')
- input_grad: bfloat16 [2048, 2048], P('fs')
- up_grad_out: float32 [2048, 4096], P('fs', 'tp')
All inputs are finite; a program needn't handle non-finite values.
Results may differ from a plain program's by a relative error of at most 0.013.
Values may be sent and summed in bfloat16 or wider, within the bound.
A program may use at most 128 MiB of HBM per device.

v0:
```python
import jax
import jax.numpy as jnp
from jax import lax
from jax.sharding import PartitionSpec as P


def per_device(fwd_input, saved_input, out_cotangent, up_weight, down_weight, up_grad_sum):
    row_count = fwd_input.shape[0]
    stacked = jnp.concatenate([fwd_input, saved_input], axis=0)
    up_whole = lax.all_gather(up_weight, "fs", axis=0, tiled=True)
    down_whole = lax.all_gather(down_weight, "fs", axis=1, tiled=True)
    pre_both = jnp.dot(stacked, up_whole, preferred_element_type=jnp.float32)
    pre_fwd = pre_both[:row_count]
    pre_bwd = pre_both[row_count:]
    positive = jnp.maximum(pre_fwd, 0.0)
    hidden = (positive * positive).astype(jnp.bfloat16)
    out_part = jnp.dot(hidden, down_whole, preferred_element_type=jnp.float32)
    layer_out = lax.psum(out_part.astype(jnp.bfloat16), "tp")
    d_hidden = lax.dot_general(
        out_cotangent, down_whole, (((1,), (1,)), ((), ())), preferred_element_type=jnp.float32
    )
    d_pre = (d_hidden * 2.0 * jnp.maximum(pre_bwd, 0.0)).astype(jnp.bfloat16)
    in_part = lax.dot_general(
        d_pre, up_whole, (((1,), (1,)), ((), ())), preferred_element_type=jnp.float32
    )
    input_grad = lax.psum(in_part.astype(jnp.bfloat16), "tp")
    grad_part = lax.psum_scatter(
        lax.dot_general(
            saved_input, d_pre, (((0,), (0,)), ((), ())), preferred_element_type=jnp.float32
        ),
        "fs",
        scatter_dimension=0,
        tiled=True,
    )
    grad_scale = float(row_count * lax.axis_size("fs")) ** (-0.5)
    return (layer_out, input_grad, up_grad_sum + grad_part * grad_scale)


def solution(mesh):
    placed = (
        P("fs", None),
        P("fs", None),
        P("fs", None),
        P("fs", "tp"),
        P("tp", "fs"),
        P("fs", "tp"),
    )
    return jax.shard_map(
        per_device,
        mesh=mesh,
        in_specs=placed,
        out_specs=(P("fs", None), P("fs", None), P("fs", "tp")),
        check_vma=False,
    )
```

profile of v0, /device:TPU:0, one launch (start us, length us, event | category | flops | bytes accessed | tf_op | source)
XLA Modules:
  0.0 666.1 jit_solution(1798604370416390500)
XLA Ops:
  7.2 0.0 copy-start
  7.2 0.0 all-gather.3.cloned.1.call-start
  7.2 0.7 all-gather.3.cloned.1.call-update
  7.9 0.0 all-gather.5.cloned.1.call-start
  8.0 0.7 all-gather.5.cloned.1.call-update
  8.7 0.0 reduce-scatter.2.cloned.1.call-start
  8.7 117.1 %all-gather.3.cloned.1.call-done = bf16[2048,2048]{1,0:T(8,128)(2,1)} async-done(((bf16[128,2048]{1,0:T(8,128)(2,1)}), bf16[2048,2048]{1,0:T(8,128)(2,1)}) %all-gather.3.cloned.1.call-update) | async-done | bytes 8388624 | tf_op jit(solution)/shard_map/all_gather | solution.py:10
  125.8 6.0 fusion.4
  131.9 136.7 %all-gather.5.cloned.1.call-done = bf16[2048,2048]{1,0:T(8,128)(2,1)} async-done(((bf16[2048,128]{1,0:T(8,128)(2,1)}), bf16[2048,2048]{1,0:T(8,128)(2,1)}) %all-gather.5.cloned.1.call-update) | async-done | bytes 8388624 | tf_op jit(solution)/shard_map/all_gather | solution.py:11
  268.6 0.0 copy-done
  268.6 6.3 fusion.1
  274.9 8.1 %convolution_bitcast_fusion = f32[2048,2048]{0,1:T(8,128)} fusion(bf16[128,2048]{1,0:T(8,128)(2,1)S(1)} %fusion.1, bf16[128,2048]{1,0:T(8,128)(2,1)S(1)} %copy-done.1), kind=kOutput, calls=%fused_computation | convolution fusion | flops 1073741824 | bytes 17825792 | tf_op jit(solution)/shard_map/dot_general | solution.py:28
  283.0 0.0 reduce-scatter.2.cloned.1.call-update
  283.0 0.0 all-reduce.3.cloned.1.call-start
  283.1 7.1 %convolution_convert_fusion = bf16[128,2048]{1,0:T(8,128)(2,1)} fusion(bf16[128,2048]{1,0:T(8,128)(2,1)S(1)} %fusion.1, bf16[2048,2048]{1,0:T(8,128)(2,1)} %all-gather.3.cloned.1.call-done), kind=kOutput, calls=%fused_computation.3 | convolution fusion | flops 1074003968 | bytes 9437184 | tf_op jit(solution)/shard_map/dot_general | solution.py:23
  290.2 5.4 convolution_convert_fusion.1
  295.6 0.0 all-reduce.3.cloned.1.call-update
  295.6 1.6 copy.9
  297.2 330.6 %reduce-scatter.2.cloned.1.call-done = f32[128,2048]{0,1:T(8,128)} async-done(((f32[2048,2048]{0,1:T(8,128)}), f32[128,2048]{0,1:T(8,128)}) %reduce-scatter.2.cloned.1.call-update) | async-done | bytes 1048592 | tf_op jit(solution)/shard_map/reduce_scatter | solution.py:27
  627.8 1.3 multiply_add_fusion
  629.2 1.3 copy.10
  630.5 25.3 %all-reduce.3.cloned.1.call-done = (bf16[128,2048]{1,0:T(8,128)(2,1)}, bf16[128,2048]{1,0:T(8,128)(2,1)}) async-done(((bf16[128,2048]{1,0:T(8,128)(2,1)}, bf16[128,2048]{1,0:T(8,128)(2,1)}), (bf16[128,2048]{1,0:T(8,128)(2,1)}, bf16[128,2048]{1,0:T(8,128)(2,1)})) %all-reduce.3.cloned.1.call-update) | async-done | bytes 1048592 | tf_op jit(solution)/shard_map/psum | solution.py:18
  655.8 1.9 copy.13
  657.7 1.9 copy.14
  (2 shorter events, 0.0 us)
Async XLA Ops:
  7.2 261.4 %copy-start = (bf16[128,2048]{1,0:T(8,128)(2,1)S(1)}, bf16[128,2048]{1,0:T(8,128)(2,1)}, u32[]{:S(2)}) copy-start(bf16[128,2048]{1,0:T(8,128)(2,1)} %param.8) | copy-start | bytes 1572868
  7.2 118.6 %all-gather.3.cloned.1.call-start = ((), (), s32[]{:S(2)}) async-start(), calls=%async_computation.1 | async-start | bytes 8912896 | tf_op jit(solution)/shard_map/all_gather | solution.py:10
  7.9 260.6 %all-gather.5.cloned.1.call-start = ((), (), s32[]{:S(2)}) async-start(), calls=%async_computation.2 | async-start | bytes 8912896 | tf_op jit(solution)/shard_map/all_gather | solution.py:11
  8.7 619.1 %reduce-scatter.2.cloned.1.call-start = ((), (), s32[]{:S(2)}) async-start(), calls=%async_computation.3 | async-start | bytes 17825792 | tf_op jit(solution)/shard_map/reduce_scatter | solution.py:27
  268.6 6.3 copy-start.1
  283.0 372.7 %all-reduce.3.cloned.1.call-start = ((), (), s32[]{:S(2)}) async-start(), calls=%async_computation.4 | async-start | bytes 2097152 | tf_op jit(solution)/shard_map/psum | solution.py:18
Sparse Core Ops, SparseCore 0:
  10.8 115.0 all-gather.2
  128.5 139.9 all-gather.4
  283.2 344.5 reduce-scatter.1
  630.6 25.1 all-reduce.2
where the time goes:
time: 666 us
  waiting for transfers between devices  611 us (92%)
  matrix products  33 us (5%)
  between operations  13.8 us (2%)
    reduce_scatter x1, waiting for transfers between devices, per_device(): lax.psum_scatter(lax.dot_general(saved_input, d_pre, (((0,), (0,)), ((),...  331 us
    all_gather x1, waiting for transfers between devices, per_device(): down_whole = lax.all_gather(down_weight, 'fs', axis=1, tiled=True)  137 us
    all_gather x1, waiting for transfers between devices, per_device(): up_whole = lax.all_gather(up_weight, 'fs', axis=0, tiled=True)  117 us
    psum x1, waiting for transfers between devices, per_device(): layer_out = lax.psum(out_part.astype(jnp.bfloat16), 'tp')  25.3 us
  transfers between devices with their start and end apart: 4, of which 4 were waited for; matrix products, arithmetic and copies ran while one was open for 3% of the time, Pallas kernels for 0%

commit v1 on v0

--- a/solution.py
+++ b/solution.py
@@ -2,13 +2,19 @@
 import jax.numpy as jnp
 from jax import lax
 from jax.sharding import PartitionSpec as P
+from jax.lax import all_gather
+
+
+def flows_prepare(content):
+    tmp = all_gather(content, "fs")
+    return jnp.concatenate(tmp, 1)
 
 
 def per_device(fwd_input, saved_input, out_cotangent, up_weight, down_weight, up_grad_sum):
     row_count = fwd_input.shape[0]
     stacked = jnp.concatenate([fwd_input, saved_input], axis=0)
     up_whole = lax.all_gather(up_weight, "fs", axis=0, tiled=True)
-    down_whole = lax.all_gather(down_weight, "fs", axis=1, tiled=True)
+    down_whole = flows_prepare(down_weight)
     pre_both = jnp.dot(stacked, up_whole, preferred_element_type=jnp.float32)
     pre_fwd = pre_both[:row_count]
     pre_bwd = pre_both[row_count:]

time: 666 us -> 638 us (0.958)
  waiting for transfers between devices: 611 us -> 574 us
  local copies, waits for them, and re-layouts: 6.63 us -> 19.1 us
    all_gather x1, waiting for transfers between devices: 137 us -> 117 us  [flows_prepare(): tmp = all_gather(content, 'fs')]
    all_gather x1, waiting for transfers between devices: 117 us -> 101 us  [per_device(): up_whole = lax.all_gather(up_weight, 'fs', axis=0, tiled=True)]
    reshape x0 -> x1, local copies, waits for them, and re-layouts: none -> 12.4 us  [flows_prepare(): return jnp.concatenate(tmp, 1)]
  transfers between devices with their start and end apart: 4 -> 4, of which waited for: 4 -> 4; matrix products, arithmetic and copies ran while one was open for 3% -> 5% of each run, Pallas kernels for 0% -> 0%
where the time goes in v1:
time: 638 us
  waiting for transfers between devices  574 us (90%)
  matrix products  29.7 us (5%)
  local copies, waits for them, and re-layouts  19.1 us (3%)
  between operations  13.8 us (2%)
    reduce_scatter x1, waiting for transfers between devices, per_device(): lax.psum_scatter(lax.dot_general(saved_input, d_pre, (((0,), (0,)), ((),...  329 us
    all_gather x1, waiting for transfers between devices, flows_prepare(): tmp = all_gather(content, 'fs')  117 us
    all_gather x1, waiting for transfers between devices, per_device(): up_whole = lax.all_gather(up_weight, 'fs', axis=0, tiled=True)  101 us
    psum x1, waiting for transfers between devices, per_device(): layer_out = lax.psum(out_part.astype(jnp.bfloat16), 'tp')  25.3 us
  transfers between devices with their start and end apart: 4, of which 4 were waited for; matrix products, arithmetic and copies ran while one was open for 5% of the time, Pallas kernels for 0%

profile of v1, /device:TPU:0, one launch (start us, length us, event | category | flops | bytes accessed | tf_op | source)
XLA Modules:
  0.0 637.8 jit_solution(6117836198412460235)
XLA Ops:
  7.2 0.0 copy-start
  7.2 0.0 all-gather.6.cloned.1.call-start
  7.2 0.7 all-gather.6.cloned.1.call-update
  7.9 0.0 all-gather.4.cloned.1.call-start
  8.0 0.7 all-gather.4.cloned.1.call-update
  8.7 0.0 reduce-scatter.2.cloned.1.call-start
  8.7 117.1 %all-gather.6.cloned.1.call-done = bf16[32768,128]{1,0:T(8,128)(2,1)} async-done(((bf16[2048,128]{1,0:T(8,128)(2,1)}), bf16[32768,128]{1,0:T(8,128)(2,1)}) %all-gather.6.cloned.1.call-update) | async-done | bytes 8388624 | tf_op jit(solution)/shard_map/all_gather | solution.py:9
  125.8 12.4 %copy.13 = bf16[2048,16,128]{0,2,1:T(8,128)(2,1)} copy(bf16[2048,16,128]{2,0,1:T(8,128)(2,1)} %bitcast.16) | data formatting | bytes 16777216 | tf_op jit(solution)/shard_map/reshape | solution.py:10
  138.2 100.9 %all-gather.4.cloned.1.call-done = bf16[2048,2048]{1,0:T(8,128)(2,1)} async-done(((bf16[128,2048]{1,0:T(8,128)(2,1)}), bf16[2048,2048]{1,0:T(8,128)(2,1)}) %all-gather.4.cloned.1.call-update) | async-done | bytes 8388624 | tf_op jit(solution)/shard_map/all_gather | solution.py:16
  239.1 6.0 fusion.4
  245.1 1.4 fusion.1
  246.6 8.1 %convolution_bitcast_fusion = f32[2048,2048]{0,1:T(8,128)} fusion(bf16[128,2048]{1,0:T(8,128)(2,1)S(1)} %fusion.1, bf16[128,2048]{1,0:T(8,128)(2,1)S(1)} %copy-done.3), kind=kOutput, calls=%fused_computation | convolution fusion | flops 1073741824 | bytes 17825792 | tf_op jit(solution)/shard_map/dot_general | solution.py:34
  254.7 0.0 reduce-scatter.2.cloned.1.call-update
  254.7 0.0 all-reduce.3.cloned.1.call-start
  254.8 7.1 %convolution_convert_fusion = bf16[128,2048]{1,0:T(8,128)(2,1)} fusion(bf16[128,2048]{1,0:T(8,128)(2,1)S(1)} %fusion.1, bf16[2048,2048]{1,0:T(8,128)(2,1)} %all-gather.4.cloned.1.call-done), kind=kOutput, calls=%fused_computation.3 | convolution fusion | flops 1074003968 | bytes 9437184 | tf_op jit(solution)/shard_map/dot_general | solution.py:29
  261.9 7.1 %convolution_convert_fusion.1 = bf16[128,2048]{1,0:T(8,128)(2,1)} fusion(bf16[2048,2048]{0,1:T(8,128)(2,1)} %bitcast.14, f32[256,2048]{1,0:T(8,128)S(1)} %fusion.4), kind=kOutput, calls=%fused_computation.4 | convolution fusion | flops 1074790400 | bytes 9961472 | tf_op jit(solution)/shard_map/dot_general | solution.py:23
  268.9 0.0 all-reduce.3.cloned.1.call-update
  268.9 1.6 copy.14
  270.5 328.9 %reduce-scatter.2.cloned.1.call-done = f32[128,2048]{0,1:T(8,128)} async-done(((f32[2048,2048]{0,1:T(8,128)}), f32[128,2048]{0,1:T(8,128)}) %reduce-scatter.2.cloned.1.call-update) | async-done | bytes 1048592 | tf_op jit(solution)/shard_map/reduce_scatter | solution.py:33
  599.5 1.3 multiply_add_fusion
  600.8 1.3 copy.15
  602.1 25.3 %all-reduce.3.cloned.1.call-done = (bf16[128,2048]{1,0:T(8,128)(2,1)}, bf16[128,2048]{1,0:T(8,128)(2,1)}) async-done(((bf16[128,2048]{1,0:T(8,128)(2,1)}, bf16[128,2048]{1,0:T(8,128)(2,1)}), (bf16[128,2048]{1,0:T(8,128)(2,1)}, bf16[128,2048]{1,0:T(8,128)(2,1)})) %all-reduce.3.cloned.1.call-update) | async-done | bytes 1048592 | tf_op jit(solution)/shard_map/psum | solution.py:24
  627.5 1.9 copy.18
  629.4 1.9 copy.19
  (7 shorter events, 0.0 us)
Async XLA Ops:
  7.2 238.0 %copy-start = (bf16[128,2048]{1,0:T(8,128)(2,1)S(1)}, bf16[128,2048]{1,0:T(8,128)(2,1)}, u32[]{:S(2)}) copy-start(bf16[128,2048]{1,0:T(8,128)(2,1)} %param.8) | copy-start | bytes 1572868
  7.2 118.6 %all-gather.6.cloned.1.call-start = ((), (), s32[]{:S(2)}) async-start(), calls=%async_computation.3 | async-start | bytes 8912896 | tf_op jit(solution)/shard_map/all_gather | solution.py:9
  7.9 231.2 %all-gather.4.cloned.1.call-start = ((), (), s32[]{:S(2)}) async-start(), calls=%async_computation.1 | async-start | bytes 8912896 | tf_op jit(solution)/shard_map/all_gather | solution.py:16
  8.7 590.8 %reduce-scatter.2.cloned.1.call-start = ((), (), s32[]{:S(2)}) async-start(), calls=%async_computation.2 | async-start | bytes 17825792 | tf_op jit(solution)/shard_map/reduce_scatter | solution.py:33
  125.8 113.3 %copy-start.2 = (bf16[128,2048]{1,0:T(8,128)(2,1)S(1)}, bf16[128,2048]{1,0:T(8,128)(2,1)}, u32[]{:S(2)}) copy-start(bf16[128,2048]{1,0:T(8,128)(2,1)} %param.7) | copy-start | bytes 1572868
  239.1 6.0 copy-start.1
  245.1 1.5 copy-start.3
  254.7 372.7 %all-reduce.3.cloned.1.call-start = ((), (), s32[]{:S(2)}) async-start(), calls=%async_computation.4 | async-start | bytes 2097152 | tf_op jit(solution)/shard_map/psum | solution.py:24
Sparse Core Ops, SparseCore 0:
  10.8 115.0 all-gather.5
  128.6 110.4 all-gather.3
  254.9 344.5 reduce-scatter.1
  602.3 25.1 all-reduce.2
